TPU v7x, 32 devices: a whole 2x2x4 slice. The times are simulated.
32 devices in a mesh: grp: 2 (over x), ep: 16 (over z, y, core).
Axes of the slice: x: 2, y: 2, z: 4, core: 2. Of those that a mesh axis runs over, the one named last changes fastest.
Arguments:
- tokens: bfloat16 [2048, 2048], P(('grp', 'ep')), parts along dimension 0, may hold values from -6 to 6
- lengths: int32 [256], P(('grp', 'ep')), parts along dimension 0, may hold values from 1 to 8, 384 in all
- experts: int32 [2048, 2], P(('grp', 'ep')), parts along dimension 0, may hold values from 0 to 3, all different within a row; in each aligned block of 64 rows (0 to 63, 64 to 127, ...) at most 64 rows name the same one
- route_weights: float32 [2048, 2], P(('grp', 'ep')), parts along dimension 0, may hold values from 0.2 to 1
- gate_proj: bfloat16 [16, 2048, 1792], P('ep'), may hold values from -0.125 to 0.125
- up_proj: bfloat16 [16, 2048, 1792], P('ep'), may hold values from -0.125 to 0.125
- down_proj: bfloat16 [16, 1792, 2048], P('ep'), may hold values from -0.0625 to 0.0625
- norm_gain: float32 [2048], replicated, may hold values from 0.1 to 1.9
- norm_bias: float32 [2048], replicated, may hold values from -3 to 3
Outputs:
- mixed: bfloat16 [2048, 2048], P(('grp', 'ep')), parts along dimension 0
There are 2 independent parts, one for each index of `grp`. A program takes and returns all parts, laid end to end along the dimension named above; an argument that names none is the same for every part. Nothing has to cross between parts.
Inputs may be any that keep to these rules, and one draw needn't show every extreme that they name: Each row names 2 different experts; in the rows of one device (aligned blocks of 64 rows) no expert is named by more than 64 rows. Within each copy of the problem the 128 lengths sum to 384; the whole array, over all copies, sums to that times the number of copies.
All inputs are finite; a program needn't handle non-finite values. No bound on the sum of `lengths` on one device may be relied on, other than what follows from the above.
Results may differ from a plain program's by a relative error of at most 0.0021.
Values may be sent and summed in bfloat16 or wider, within the bound.
A program may use at most 128 MiB of HBM per device.

v0:
```python
import jax
import jax.numpy as jnp
from jax import lax
from jax.sharding import PartitionSpec as P

SPLIT = 4
TOP = 2
SPAN = 8
RESIDUAL_SCALE = 8.0**0.25
NORM_EPS = 1e-05


def layer_norm(values, norm_gain, norm_bias):
    center = values - jnp.mean(values, -1, keepdims=True)
    variance = jnp.mean(center * center, -1, keepdims=True)
    return center * lax.rsqrt(variance + NORM_EPS) * norm_gain + norm_bias


def expert_rows(picked, gate_proj, up_proj, down_proj):
    pre_gate = jnp.dot(picked, gate_proj[0], preferred_element_type=jnp.float32)
    pre_up = jnp.dot(picked, up_proj[0], preferred_element_type=jnp.float32)
    hidden = (jax.nn.silu(pre_gate) * pre_up).astype(jnp.bfloat16)
    return jnp.dot(hidden, down_proj[0], preferred_element_type=jnp.float32)


def local(
    tokens, lengths, experts, route_weights, gate_proj, up_proj, down_proj, norm_gain, norm_bias
):
    slot_count, width = tokens.shape
    axis_count = lax.axis_size("ep")
    capacity = 2 * slot_count * TOP * SPLIT // axis_count
    position = jnp.arange(slot_count, dtype=jnp.int32)
    alive_mask = position % SPAN < jnp.repeat(lengths, SPAN, total_repeat_length=slot_count)
    inputs = tokens.astype(jnp.float32)
    gathered = lax.all_gather(tokens, "ep", axis=0, tiled=True)
    all_experts, all_lengths = (
        lax.all_gather(experts, "ep", axis=0, tiled=True),
        lax.all_gather(lengths, "ep", axis=0, tiled=True),
    )
    all_weights = lax.all_gather(route_weights, "ep", axis=0, tiled=True)
    total_slots = gathered.shape[0]
    all_position = jnp.arange(total_slots, dtype=jnp.int32)
    all_alive = all_position % SPAN < jnp.repeat(all_lengths, SPAN, total_repeat_length=total_slots)
    own_expert = lax.axis_index("ep") // SPLIT
    hits = (all_experts == own_expert) & all_alive[:, None]
    chosen = hits.reshape(total_slots * TOP).astype(jnp.int32)
    order_rank = jnp.cumsum(chosen) - 1
    row_count = axis_count * capacity
    rows_index = jnp.arange(row_count, dtype=jnp.int32)
    picker = (order_rank[None, :] == rows_index[:, None]) & (chosen[None, :] == 1)
    flat_slot = jnp.repeat(all_position, TOP, total_repeat_length=total_slots * TOP)
    row_source = jnp.sum(jnp.where(picker, flat_slot[None, :], 0), axis=1)
    picked = jnp.take(gathered, row_source, axis=0)
    results = expert_rows(picked, gate_proj, up_proj, down_proj)
    rank_pairs = order_rank.reshape(total_slots, TOP)
    slot_row = jnp.sum(jnp.where(hits, rank_pairs, 0), axis=1)
    slot_weight = jnp.sum(jnp.where(hits, all_weights, 0.0), axis=1)
    spread_back = jnp.take(results, slot_row, axis=0) * slot_weight[:, None]
    branch = lax.psum_scatter(spread_back, "ep", scatter_dimension=0, tiled=True)
    normed = layer_norm(RESIDUAL_SCALE * inputs + branch, norm_gain, norm_bias)
    return jnp.where(alive_mask[:, None], normed, 0.0).astype(jnp.bfloat16)


def solution(mesh):
    in_specs = (
        P(("grp", "ep"), None),
        P(("grp", "ep")),
        P(("grp", "ep"), None),
        P(("grp", "ep"), None),
        P("ep", None, None),
        P("ep", None, None),
        P("ep", None, None),
        P(),
        P(),
    )
    out_specs = P(("grp", "ep"), None)
    return jax.shard_map(local, mesh=mesh, in_specs=in_specs, out_specs=out_specs, check_vma=False)
```

profile of v0, /device:TPU:0, one launch (start us, length us, event | category | flops | bytes accessed | tf_op | source)
XLA Modules:
  0.0 260.8 jit_solution(14044084314716863981)
XLA Ops:
  6.5 0.0 all-gather.4.cloned.1.call-start
  6.5 0.7 all-gather.4.cloned.1.call-update
  7.3 0.0 reduce-scatter.2.cloned.1.call-start
  7.3 23.6 %all-gather = s32[16,64,2]{1,2,0:T(2,128)S(1)} all-gather(s32[1,64,2]{1,2,0:T(2,128)} %bitcast.52), channel_id=1, replica_groups=mesh['grp'=2,'ep'=16] {'ep'}, dimensions={0}, use_global_device_ids=true | all-gather | bytes 8704 | tf_op jit(solution)/shard_map/all_gather | solution.py:37
  30.9 0.1 reshape.405
  31.0 1.2 dynamic-slice.18
  32.9 0.9 dynamic-update-slice.8
  33.8 7.1 %all-reduce = s32[128]{0:T(128)S(1)} all-reduce(s32[128]{0:T(128)S(1)} %dynamic-update-slice.8), channel_id=1, replica_groups=mesh['grp'=2,'ep'=16] {'ep'}, use_global_device_ids=true, to_apply=%add | all-reduce | flops 128 | bytes 1024
  40.9 0.8 add_add_fusion.1
  41.7 6.6 %gather_fusion = s32[1024]{0:T(1024)S(1)} fusion(s32[128]{0:T(128)S(1)} %all-reduce, s32[1024]{0:T(1024)S(1)} %broadcast_clamp_fusion.2), kind=kCustom, calls=%fused_computation | custom fusion | bytes 12288 | tf_op jit(solution)/shard_map/jit(_take)/gather | solution.py:43
  48.3 0.8 fusion.12
  49.0 0.2 copy.26
  49.3 0.3 reshape.357
  49.5 0.3 reduce-window.23
  49.8 0.1 slice.72
  49.9 0.5 reshape.354
  50.4 23.2 %all-gather.1 = f32[16,64,2]{1,2,0:T(2,128)S(1)} all-gather(f32[1,64,2]{1,2,0:T(2,128)} %bitcast.53), channel_id=1, replica_groups=mesh['grp'=2,'ep'=16] {'ep'}, dimensions={0}, use_global_device_ids=true | all-gather | bytes 8704 | tf_op jit(solution)/shard_map/all_gather | solution.py:40
  73.6 0.1 reshape.403
  73.7 0.3 copy.28
  73.9 0.4 eq.44
  74.3 0.1 slice_reduce_fusion
  74.4 0.1 broadcast.380
  74.5 0.1 reshape.356
  74.6 0.2 copy.27
  74.9 0.1 add_bitcast_fusion
  74.9 2.5 select_reduce_fusion
  77.5 0.0 all-gather.4.cloned.1.call-done
  77.5 11.7 %gather_fusion.1 = bf16[1024,2048]{1,0:T(8,128)(2,1)} fusion(bf16[1024,2048]{1,0:T(8,128)(2,1)} %all-gather.4.cloned.1.call-done, s32[1024]{0:T(1024)S(1)} %broadcast_clamp_fusion.1), kind=kCustom, calls=%fused_computation.1 | custom fusion | bytes 8392704 | tf_op jit(solution)/shard_map/jit(_take)/gather | solution.py:53
  89.3 13.9 %fusion.5 = f32[1024,1792]{1,0:T(8,128)} fusion(bf16[1,2048,1792]{2,1,0:T(8,128)(2,1)} %param.19, bf16[1024,2048]{1,0:T(8,128)(2,1)} %gather_fusion.1, pred[1024]{0:T(1024)(128)(4,1)S(1)} %compare_and_fusion), kind=kOutput, calls=%fused_computation.11 | convolution fusion | flops 7518289920 | bytes 18875392 | tf_op jit(solution)/shard_map/dot_general | solution.py:20
  103.1 26.9 %fusion.1 = f32[1024,2048]{1,0:T(8,128)} fusion(bf16[1,1792,2048]{2,1,0:T(8,128)(2,1)} %param.21, f32[1024,1792]{1,0:T(8,128)} %fusion.5, bf16[1,2048,1792]{2,1,0:T(8,128)(2,1)} %param.20, bf16[1024,2048]{1,0:T(8,128)(2,1)} %gather_fusion.1, pred[1024]{0:T(1024)(128)(4,1)S(1)} %compare_and_fusion), kind=kOutput, calls=%fused_computation.7 | convolution fusion | flops 15045492736 | bytes 34604032 | tf_op jit(solution)/shard_map/dot_general | solution.py:23
  130.1 12.5 %gather_fusion.2 = f32[1024,2048]{1,0:T(8,128)} fusion(f32[1024,2048]{1,0:T(8,128)} %fusion.1, s32[1024]{0:T(1024)S(1)} %broadcast_clamp_fusion), kind=kCustom, calls=%fused_computation.2 | custom fusion | bytes 16781312 | tf_op jit(solution)/shard_map/jit(_take)/gather | solution.py:58
  142.5 6.0 %select_multiply_fusion = f32[1024,2048]{1,0:T(8,128)} fusion(f32[1024,2048]{1,0:T(8,128)} %gather_fusion.2, f32[1024]{0:T(1024)S(1)} %select_reduce_fusion.1, pred[1024]{0:T(1024)(128)(4,1)S(1)} %compare_and_fusion.1), kind=kLoop, calls=%fused_computation.3 | loop fusion | flops 4194304 | bytes 16782336 | tf_op jit(solution)/shard_map/mul | solution.py:58
  148.5 0.0 copy-start.7
  148.5 0.0 copy-start.8
  148.5 0.0 copy-start.9
  148.5 0.0 copy-start.10
  148.6 0.0 copy-start
  148.6 0.0 copy-start.2
  148.6 0.0 copy-start.3
  148.6 0.0 reduce-scatter.2.cloned.1.call-update
  148.6 0.5 copy-done.1
  149.1 0.7 fusion.22
  149.8 0.0 copy-done.4
  149.9 5.1 %fusion.16 = pred[64]{0:T(512)(128)(4,1)S(1)} fusion(pred[64]{0:T(512)(128)(4,1)S(1)} %copy-done.10, pred[64]{0:T(512)(128)(4,1)S(1)} %copy-done.9, pred[64]{0:T(512)(128)(4,1)S(1)} %copy-done.8, pred[64]{0:T(512)(128)(4,1)S(1)} %copy-done.7, pred[64]{0:T(512)(128)(4,1)S(1)} %copy-done.6, pred[64]{0:T(512)(128)(4,1)S(1)} %copy-done.5, ...), kind=kLoop, calls=%fused_computation.46 | loop fusion | flops 896 | bytes 544 | tf_op jit(solution)/shard_map/lt | solution.py:33
  154.9 94.5 %reduce-scatter.2.cloned.1.call-done = f32[64,2048]{1,0:T(8,128)} async-done(((f32[1024,2048]{1,0:T(8,128)}), f32[64,2048]{1,0:T(8,128)}) %reduce-scatter.2.cloned.1.call-update) | async-done | bytes 524304 | tf_op jit(solution)/shard_map/reduce_scatter | solution.py:59
  249.5 1.2 fusion.11
  250.7 1.3 multiply_reduce_fusion
  252.0 1.9 select_convert_fusion
  (31 shorter events, 0.2 us)
Async XLA Ops:
  6.5 71.0 %all-gather.4.cloned.1.call-start = ((), (), s32[]{:S(2)}) async-start(), calls=%async_computation.1 | async-start | bytes 4456448 | tf_op jit(solution)/shard_map/all_gather | solution.py:35
  7.3 242.2 %reduce-scatter.2.cloned.1.call-start = ((), (), s32[]{:S(2)}) async-start(), calls=%async_computation.2 | async-start | bytes 8912896 | tf_op jit(solution)/shard_map/reduce_scatter | solution.py:59
  148.5 0.7 copy-start.1
  148.5 1.3 copy-start.4
  148.5 1.3 copy-start.5
  148.5 1.3 copy-start.6
  148.5 1.3 copy-start.7
  148.5 1.3 copy-start.8
  148.5 1.3 copy-start.9
  148.5 1.3 copy-start.10
  148.6 100.9 %copy-start = (bf16[64,2048]{1,0:T(8,128)(2,1)S(1)}, bf16[64,2048]{1,0:T(8,128)(2,1)}, u32[]{:S(2)}) copy-start(bf16[64,2048]{1,0:T(8,128)(2,1)} %param.15) | copy-start | bytes 786436
  148.6 103.4 %copy-start.2 = (f32[2048]{0:T(1024)S(1)}, f32[2048]{0:T(1024)}, u32[]{:S(2)}) copy-start(f32[2048]{0:T(1024)} %param.23) | copy-start | bytes 24580
  148.6 103.4 %copy-start.3 = (f32[2048]{0:T(1024)S(1)}, f32[2048]{0:T(1024)}, u32[]{:S(2)}) copy-start(f32[2048]{0:T(1024)} %param.22) | copy-start | bytes 24580
Sparse Core Ops, SparseCore 0:
  9.5 53.3 all-gather.3
  148.7 100.6 reduce-scatter.1
where the time goes:
time: 261 us
  waiting for transfers between devices  95.3 us (37%)
  blocking collectives  53.9 us (21%)
  matrix products  40.8 us (16%)
  local copies, waits for them, and re-layouts  36.4 us (14%)
  other arithmetic  20 us (8%)
  between operations  14.3 us (5%)
    reduce_scatter x1, waiting for transfers between devices, local(): lax.psum_scatter(spread_back, 'ep', scatter_dimension=0, tiled=True)  94.5 us
    dot_general x1, matrix products, expert_rows(): return jnp.dot(hidden, down_proj[0], preferred_element_type=jnp.float32)  26.9 us
    all_gather x1, blocking collectives, local(): lax.all_gather(experts, 'ep', axis=0, tiled=True)  23.6 us
    all_gather x1, blocking collectives, local(): all_weights = lax.all_gather(route_weights, 'ep', axis=0, tiled=True)  23.2 us
    dot_general x1, matrix products, expert_rows(): pre_gate = jnp.dot(picked, gate_proj[0], preferred_element_type=jnp.float32)  13.9 us
    gather x1, local copies, waits for them, and re-layouts, local(): spread_back = jnp.take(results, slot_row, axis=0) * slot_weight[:, None]  12.5 us
    gather x1, local copies, waits for them, and re-layouts, local(): picked = jnp.take(gathered, row_source, axis=0)  11.7 us
    unnamed x1, blocking collectives  7.11 us
  transfers between devices with their start and end apart: 2, of which 1 were waited for; matrix products, arithmetic and copies ran while one was open for 8% of the time, Pallas kernels for 0%

commit v1 on v0

--- a/solution.py
+++ b/solution.py
@@ -32,12 +32,15 @@
     position = jnp.arange(slot_count, dtype=jnp.int32)
     alive_mask = position % SPAN < jnp.repeat(lengths, SPAN, total_repeat_length=slot_count)
     inputs = tokens.astype(jnp.float32)
-    gathered = lax.all_gather(tokens, "ep", axis=0, tiled=True)
     all_experts, all_lengths = (
         lax.all_gather(experts, "ep", axis=0, tiled=True),
         lax.all_gather(lengths, "ep", axis=0, tiled=True),
     )
-    all_weights = lax.all_gather(route_weights, "ep", axis=0, tiled=True)
+    gathered, all_weights = jnp.split(
+        lax.all_gather(jnp.concatenate([tokens, route_weights], axis=1), "ep", axis=0, tiled=True),
+        [tokens.shape[1]],
+        axis=1,
+    )
     total_slots = gathered.shape[0]
     all_position = jnp.arange(total_slots, dtype=jnp.int32)
     all_alive = all_position % SPAN < jnp.repeat(all_lengths, SPAN, total_repeat_length=total_slots)

time: 261 us -> 283 us (1.084)
  waiting for transfers between devices: 95.3 us -> 130 us
  blocking collectives: 53.9 us -> 31 us
  local copies, waits for them, and re-layouts: 36.4 us -> 42.4 us
  other arithmetic: 20 us -> 23.3 us
    all_gather x1, waiting for transfers between devices: 0.02 us -> 34.3 us  [local(): lax.all_gather(jnp.concatenate([tokens, route_weights], axis=1), 'ep', ax...]
    all_gather x1 -> x0, blocking collectives: 23.2 us -> none  [local(): all_weights = lax.all_gather(route_weights, 'ep', axis=0, tiled=True)]
    split x0 -> x1, local copies, waits for them, and re-layouts: none -> 6.03 us  [local(): jnp.split(lax.all_gather(jnp.concatenate([tokens, route_weights], axis=1)...]
  transfers between devices with their start and end apart: 2 -> 2, of which waited for: 1 -> 2; matrix products, arithmetic and copies ran while one was open for 8% -> 7% of each run, Pallas kernels for 0% -> 0%
where the time goes in v1:
time: 283 us; the launch traced here: 282 us
  waiting for transfers between devices  130 us (46%)
  local copies, waits for them, and re-layouts  42.4 us (15%)
  matrix products  41 us (14%)
  blocking collectives  31 us (11%)
  other arithmetic  23.3 us (8%)
  between operations  14.3 us (5%)
    reduce_scatter x1, waiting for transfers between devices, local(): lax.psum_scatter(spread_back, 'ep', scatter_dimension=0, tiled=True)  95.7 us
    all_gather x1, waiting for transfers between devices, local(): lax.all_gather(jnp.concatenate([tokens, route_weights], axis=1), 'ep', ax...  34.3 us
    dot_general x1, matrix products, expert_rows(): return jnp.dot(hidden, down_proj[0], preferred_element_type=jnp.float32)  27 us
    all_gather x1, blocking collectives, local(): lax.all_gather(experts, 'ep', axis=0, tiled=True)  23.8 us
    dot_general x1, matrix products, expert_rows(): pre_gate = jnp.dot(picked, gate_proj[0], preferred_element_type=jnp.float32)  14 us
    gather x1, local copies, waits for them, and re-layouts, local(): spread_back = jnp.take(results, slot_row, axis=0) * slot_weight[:, None]  12.4 us
    gather x1, local copies, waits for them, and re-layouts, local(): picked = jnp.take(gathered, row_source, axis=0)  11.5 us
    unnamed x1, blocking collectives  7.23 us
  transfers between devices with their start and end apart: 2, of which 2 were waited for; matrix products, arithmetic and copies ran while one was open for 7% of the time, Pallas kernels for 0%

profile of v1, /device:TPU:0, one launch (start us, length us, event | category | flops | bytes accessed | tf_op | source)
XLA Modules:
  0.0 282.1 jit_solution(4689585024295363372)
XLA Ops:
  6.5 0.8 copy.20
  7.3 1.0 convert_element_type.24
  8.3 0.9 pad_maximum_fusion
  9.2 0.0 all-gather.3.cloned.1.call-update
  9.2 0.0 reduce-scatter.2.cloned.1.call-start
  9.3 23.8 %all-gather = s32[16,64,2]{1,2,0:T(2,128)S(1)} all-gather(s32[1,64,2]{1,2,0:T(2,128)} %bitcast.49), channel_id=1, replica_groups=mesh['grp'=2,'ep'=16] {'ep'}, dimensions={0}, use_global_device_ids=true | all-gather | bytes 8704 | tf_op jit(solution)/shard_map/all_gather | solution.py:36
  33.1 0.3 copy.21
  33.4 1.2 dynamic-slice.18
  35.3 0.9 dynamic-update-slice.8
  36.2 7.2 %all-reduce = s32[128]{0:T(128)S(1)} all-reduce(s32[128]{0:T(128)S(1)} %dynamic-update-slice.8), channel_id=1, replica_groups=mesh['grp'=2,'ep'=16] {'ep'}, use_global_device_ids=true, to_apply=%add | all-reduce | flops 128 | bytes 1024
  43.4 0.8 add_add_fusion.1
  44.2 6.6 %gather_fusion = s32[1024]{0:T(1024)S(1)} fusion(s32[128]{0:T(128)S(1)} %all-reduce, s32[1024]{0:T(1024)S(1)} %broadcast_clamp_fusion), kind=kCustom, calls=%fused_computation.2 | custom fusion | bytes 12288 | tf_op jit(solution)/shard_map/jit(_take)/gather | solution.py:46
  50.8 0.8 fusion.25
  51.5 0.2 broadcast_compare_fusion
  51.8 0.3 reshape.326
  52.0 0.3 reduce-window.23
  52.3 0.1 slice.72
  52.4 0.5 reshape.324
  52.9 0.3 eq.44
  53.2 0.1 slice_reduce_fusion
  53.4 0.1 broadcast.337
  53.4 0.1 reshape.325
  53.5 0.5 select_reduce_fusion.1
  54.0 0.1 add_bitcast_fusion
  54.1 1.8 select_reduce_fusion
  55.9 34.3 %all-gather.3.cloned.1.call-done = f32[1024,2050]{1,0:T(8,128)} async-done(((f32[64,2050]{1,0:T(8,128)}), f32[1024,2050]{1,0:T(8,128)}) %all-gather.3.cloned.1.call-update) | async-done | bytes 8396816 | tf_op jit(solution)/shard_map/all_gather | solution.py:40
  90.2 6.0 %split.8 = bf16[1024,2048]{1,0:T(8,128)(2,1)} slice(f32[1024,2050]{1,0:T(8,128)} %all-gather.3.cloned.1.call-done), slice={[0:1024], [0:2048]} | slice | bytes 8388608 | tf_op jit(solution)/shard_map/split | solution.py:39
  96.2 11.5 %gather_fusion.1 = bf16[1024,2048]{1,0:T(8,128)(2,1)} fusion(bf16[1024,2048]{1,0:T(8,128)(2,1)} %split.8, s32[1024]{0:T(1024)S(1)} %fusion.29), kind=kCustom, calls=%fused_computation.clone | custom fusion | bytes 8392704 | tf_op jit(solution)/shard_map/jit(_take)/gather | solution.py:56
  107.7 14.0 %fusion.3 = f32[1024,1792]{1,0:T(8,128)} fusion(bf16[1024,2048]{1,0:T(8,128)(2,1)} %gather_fusion.1, bf16[1,2048,1792]{2,1,0:T(8,128)(2,1)} %param.21, pred[1024]{0:T(1024)(128)(4,1)S(1)} %compare_and_fusion.1), kind=kOutput, calls=%fused_computation.9 | convolution fusion | flops 7518289920 | bytes 18875392 | tf_op jit(solution)/shard_map/dot_general | solution.py:20
  121.7 27.0 %fusion.5 = f32[1024,2048]{1,0:T(8,128)} fusion(bf16[1,1792,2048]{2,1,0:T(8,128)(2,1)} %param.23, f32[1024,1792]{1,0:T(8,128)} %fusion.3, bf16[1,2048,1792]{2,1,0:T(8,128)(2,1)} %param.22, bf16[1024,2048]{1,0:T(8,128)(2,1)} %gather_fusion.1, pred[1024]{0:T(1024)(128)(4,1)S(1)} %compare_and_fusion.1), kind=kOutput, calls=%fused_computation.11 | convolution fusion | flops 15045492736 | bytes 34604032 | tf_op jit(solution)/shard_map/dot_general | solution.py:23
  148.8 12.4 %gather_fusion.2 = f32[1024,2048]{1,0:T(8,128)} fusion(f32[1024,2048]{1,0:T(8,128)} %fusion.5, s32[1024]{0:T(1024)S(1)} %fusion.30), kind=kCustom, calls=%fused_computation.1.clone | custom fusion | bytes 16781312 | tf_op jit(solution)/shard_map/jit(_take)/gather | solution.py:61
  161.2 1.4 fusion.22
  162.6 6.0 %select_multiply_fusion = f32[1024,2048]{1,0:T(8,128)} fusion(f32[1024,2048]{1,0:T(8,128)} %gather_fusion.2, f32[1024]{0:T(1024)S(1)} %fusion.22, pred[1024]{0:T(1024)(128)(4,1)S(1)} %compare_and_fusion), kind=kLoop, calls=%fused_computation.3 | loop fusion | flops 4194304 | bytes 16782336 | tf_op jit(solution)/shard_map/mul | solution.py:61
  168.7 0.0 copy-start.7
  168.7 0.0 copy-start.8
  168.7 0.0 copy-start.9
  168.7 0.0 copy-start.10
  168.7 0.0 copy-start
  168.7 0.0 copy-start.2
  168.7 0.0 copy-start.3
  168.8 0.0 reduce-scatter.2.cloned.1.call-update
  168.8 0.5 copy-done.1
  169.3 0.7 fusion.36
  170.0 5.1 %fusion.31 = pred[64]{0:T(512)(128)(4,1)S(1)} fusion(pred[64]{0:T(512)(128)(4,1)S(1)} %copy-done.10, pred[64]{0:T(512)(128)(4,1)S(1)} %copy-done.9, pred[64]{0:T(512)(128)(4,1)S(1)} %copy-done.8, pred[64]{0:T(512)(128)(4,1)S(1)} %copy-done.7, pred[64]{0:T(512)(128)(4,1)S(1)} %copy-done.6, pred[64]{0:T(512)(128)(4,1)S(1)} %copy-done.5, ...), kind=kLoop, calls=%fused_computation.53 | loop fusion | flops 896 | bytes 544 | tf_op jit(solution)/shard_map/lt | solution.py:33
  175.1 95.7 %reduce-scatter.2.cloned.1.call-done = f32[64,2048]{1,0:T(8,128)} async-done(((f32[1024,2048]{1,0:T(8,128)}), f32[64,2048]{1,0:T(8,128)}) %reduce-scatter.2.cloned.1.call-update) | async-done | bytes 524304 | tf_op jit(solution)/shard_map/reduce_scatter | solution.py:62
  270.8 1.2 fusion.24
  272.1 1.3 multiply_reduce_fusion
  273.4 1.9 select_convert_fusion
  (29 shorter events, 0.1 us)
Async XLA Ops:
  6.5 47.6 %copy-start.11 = (s32[2048]{0:T(1024)S(1)}, s32[2048]{0:T(1024)}, u32[]{:S(2)}) copy-start(s32[2048]{0:T(1024)} %constant.313.clone.1) | copy-start | bytes 24580
  6.5 83.6 %all-gather.3.cloned.1.call-start = ((), (), s32[]{:S(2)}) async-start(), calls=%async_computation.1 | async-start | bytes 9469952 | tf_op jit(solution)/shard_map/all_gather | solution.py:40
  9.2 261.6 %reduce-scatter.2.cloned.1.call-start = ((), (), s32[]{:S(2)}) async-start(), calls=%async_computation.2 | async-start | bytes 8912896 | tf_op jit(solution)/shard_map/reduce_scatter | solution.py:62
  168.7 0.7 copy-start.1
  168.7 1.3 copy-start.4
  168.7 1.3 copy-start.5
  168.7 1.3 copy-start.6
  168.7 1.3 copy-start.7
  168.7 1.3 copy-start.8
  168.7 1.3 copy-start.9
  168.7 1.3 copy-start.10
  168.7 102.1 %copy-start = (bf16[64,2048]{1,0:T(8,128)(2,1)S(1)}, bf16[64,2048]{1,0:T(8,128)(2,1)}, u32[]{:S(2)}) copy-start(bf16[64,2048]{1,0:T(8,128)(2,1)} %param.17) | copy-start | bytes 786436
  168.7 104.6 %copy-start.2 = (f32[2048]{0:T(1024)S(1)}, f32[2048]{0:T(1024)}, u32[]{:S(2)}) copy-start(f32[2048]{0:T(1024)} %param.25) | copy-start | bytes 24580
  168.7 104.6 %copy-start.3 = (f32[2048]{0:T(1024)S(1)}, f32[2048]{0:T(1024)}, u32[]{:S(2)}) copy-start(f32[2048]{0:T(1024)} %param.24) | copy-start | bytes 24580
Sparse Core Ops, SparseCore 0:
  9.6 80.5 all-gather.2
  168.9 101.8 reduce-scatter.1
